TPU v7x, 32 devices: a whole 2x2x4 slice. The times are simulated.
32 devices in a mesh: rep: 2 (over x), fs: 8 (over z, y), tp: 2 (over core).
Axes of the slice: x: 2, y: 2, z: 4, core: 2. Of those that a mesh axis runs over, the one named last changes fastest.
Arguments:
- tokens: bfloat16 [5120, 2048], P(('rep', 'fs')), may hold values from -6 to 6
- mixer_out: bfloat16 [5120, 2048], P(('rep', 'fs')), may hold values from -6 to 6
- gate_first: bfloat16 [2048, 2816], P('fs', 'tp'), may hold values from -0.125 to 0.125
- up_first: bfloat16 [2048, 2816], P('fs', 'tp'), may hold values from -0.125 to 0.125
- down_first: bfloat16 [2816, 2048], P('tp', 'fs'), may hold values from -0.3125 to 0.3125
- gate_second: bfloat16 [2048, 2816], P('fs', 'tp'), may hold values from -0.125 to 0.125
- up_second: bfloat16 [2048, 2816], P('fs', 'tp'), may hold values from -0.125 to 0.125
- down_second: bfloat16 [2816, 2048], P('tp', 'fs'), may hold values from -0.3125 to 0.3125
- gain_first: float32 [2048], replicated, may hold values from 0.1 to 1.9
- bias_first: float32 [2048], replicated, may hold values from -1.5 to 1.5
- gain_middle: float32 [2048], replicated, may hold values from 0.1 to 1.9
- bias_middle: float32 [2048], replicated, may hold values from -1.5 to 1.5
- gain_last: float32 [2048], replicated, may hold values from 0.1 to 1.9
- bias_last: float32 [2048], replicated, may hold values from -1.5 to 1.5
Outputs:
- layer_out: bfloat16 [5120, 2048], P(('rep', 'fs'))
All inputs are finite; a program needn't handle non-finite values.
Results may differ from a plain program's by a relative error of at most 0.014.
Values may be sent and summed in bfloat16 or wider, within the bound.
A program may use at most 64 MiB of HBM per device.

v0:
```python
import math
import jax
import jax.numpy as jnp
from jax import lax
from jax.sharding import PartitionSpec as P

residual_scale = math.sqrt(2.0)
norm_eps = 1e-05


def normalize(summed, scaling, offset):
    center = summed - jnp.mean(summed, axis=-1, keepdims=True)
    spread = jnp.mean(center * center, axis=-1, keepdims=True)
    return center * lax.rsqrt(spread + norm_eps) * scaling + offset


def add_columns(inputs, portion):
    return jnp.dot(inputs, portion, preferred_element_type=jnp.float32)


def project_in(inputs, gate_weight, up_weight):
    return (
        add_columns(inputs, lax.all_gather(gate_weight, "fs", axis=0, tiled=True)),
        add_columns(inputs, lax.all_gather(up_weight, "fs", axis=0, tiled=True)),
    )


def project_out(hidden, down_weight):
    return jnp.dot(
        hidden,
        lax.all_gather(down_weight, "fs", axis=1, tiled=True),
        preferred_element_type=jnp.float32,
    )


def half_step(inputs, gate_weight, up_weight, down_weight):
    gate, value = project_in(inputs, gate_weight, up_weight)
    hidden = (jax.nn.silu(gate) * value).astype(jnp.bfloat16)
    partials = project_out(hidden, down_weight)
    summed = lax.psum(partials.astype(jnp.bfloat16), "tp")
    return summed


def per_device(
    tokens,
    mixer_out,
    gate_first,
    up_first,
    down_first,
    gate_second,
    up_second,
    down_second,
    gain_first,
    bias_first,
    gain_middle,
    bias_middle,
    gain_last,
    bias_last,
):
    first_branch = half_step(tokens, gate_first, up_first, down_first)
    first_norm = normalize(
        residual_scale * tokens.astype(jnp.float32) + 0.5 * first_branch.astype(jnp.float32),
        gain_first,
        bias_first,
    ).astype(jnp.bfloat16)
    middle_norm = normalize(
        residual_scale * first_norm.astype(jnp.float32) + mixer_out.astype(jnp.float32),
        gain_middle,
        bias_middle,
    ).astype(jnp.bfloat16)
    second_branch = half_step(middle_norm, gate_second, up_second, down_second)
    finished = normalize(
        residual_scale * middle_norm.astype(jnp.float32) + 0.5 * second_branch.astype(jnp.float32),
        gain_last,
        bias_last,
    ).astype(jnp.bfloat16)
    return finished


def solution(mesh):
    return jax.shard_map(
        per_device,
        mesh=mesh,
        in_specs=(
            P(("rep", "fs"), None),
            P(("rep", "fs"), None),
            P("fs", "tp"),
            P("fs", "tp"),
            P("tp", "fs"),
            P("fs", "tp"),
            P("fs", "tp"),
            P("tp", "fs"),
            P(),
            P(),
            P(),
            P(),
            P(),
            P(),
        ),
        out_specs=P(("rep", "fs"), None),
        check_vma=False,
    )
```

profile of v0, /device:TPU:0, one launch (start us, length us, event | category | flops | bytes accessed | tf_op | source)
XLA Modules:
  0.0 639.6 jit_solution(13720102844049315975)
XLA Ops:
  6.5 0.7 all-gather.7.cloned.1.call-update
  7.3 0.7 all-gather.11.cloned.1.call-update
  8.0 0.0 all-gather.9.cloned.1.call-start
  8.1 0.7 all-gather.9.cloned.1.call-update
  8.8 0.0 all-reduce.3.cloned.1.call-start
  8.8 95.8 %all-gather.7.cloned.1.call-done = bf16[2048,1408]{1,0:T(8,128)(2,1)} async-done(((bf16[256,1408]{1,0:T(8,128)(2,1)}), bf16[2048,1408]{1,0:T(8,128)(2,1)}) %all-gather.7.cloned.1.call-update) | async-done | bytes 5767184 | tf_op jit(solution)/shard_map/all_gather | solution.py:23
  104.6 5.2 fusion.7
  109.8 88.2 %all-gather.11.cloned.1.call-done = bf16[1408,2048]{1,0:T(8,128)(2,1)} async-done(((bf16[1408,256]{1,0:T(8,128)(2,1)}), bf16[1408,2048]{1,0:T(8,128)(2,1)}) %all-gather.11.cloned.1.call-update) | async-done | bytes 5767184 | tf_op jit(solution)/shard_map/all_gather | solution.py:31
  198.0 92.7 %all-gather.9.cloned.1.call-done = bf16[2048,1408]{1,0:T(8,128)(2,1)} async-done(((bf16[256,1408]{1,0:T(8,128)(2,1)}), bf16[2048,1408]{1,0:T(8,128)(2,1)}) %all-gather.9.cloned.1.call-update) | async-done | bytes 5767184 | tf_op jit(solution)/shard_map/all_gather | solution.py:24
  290.7 9.7 %convolution_convert_fusion.1 = bf16[320,2048]{1,0:T(8,128)(2,1)} fusion(bf16[1408,2048]{1,0:T(8,128)(2,1)} %all-gather.11.cloned.1.call-done, bf16[320,2048]{1,0:T(8,128)(2,1)S(1)} %copy-done.2, bf16[2048,1408]{1,0:T(8,128)(2,1)} %all-gather.9.cloned.1.call-done, f32[320,1408]{1,0:T(8,128)S(1)} %fusion.7), kind=kOutput, calls=%fused_computation.3 | convolution fusion | flops 3694346240 | bytes 15958016 | tf_op jit(solution)/shard_map/dot_general | solution.py:29
  300.4 0.0 all-gather.13.cloned.1.call-start
  300.4 0.5 all-gather.13.cloned.1.call-update
  301.0 0.0 all-gather.15.cloned.1.call-start
  301.0 0.5 all-gather.15.cloned.1.call-update
  301.5 0.0 all-gather.17.cloned.1.call-start
  301.6 0.7 all-gather.17.cloned.1.call-update
  302.3 0.2 all-reduce.5.cloned.1.call-start
  302.5 16.1 %all-reduce.3.cloned.1.call-done = bf16[320,2048]{1,0:T(8,128)(2,1)} async-done(((bf16[320,2048]{1,0:T(8,128)(2,1)}), bf16[320,2048]{1,0:T(8,128)(2,1)}) %all-reduce.3.cloned.1.call-update) | async-done | bytes 1310736 | tf_op jit(solution)/shard_map/psum | solution.py:40
  318.6 2.0 fusion.3
  320.6 0.8 multiply_reduce_fusion.2
  321.5 1.3 fusion.2
  322.8 0.7 multiply_reduce_fusion.1
  323.5 0.8 add_convert_fusion.1
  324.3 89.9 %all-gather.13.cloned.1.call-done = bf16[2048,1408]{1,0:T(8,128)(2,1)} async-done(((bf16[256,1408]{1,0:T(8,128)(2,1)}), bf16[2048,1408]{1,0:T(8,128)(2,1)}) %all-gather.13.cloned.1.call-update) | async-done | bytes 5767184 | tf_op jit(solution)/shard_map/all_gather | solution.py:23
  414.2 4.8 fusion.8
  419.0 87.7 %all-gather.15.cloned.1.call-done = bf16[2048,1408]{1,0:T(8,128)(2,1)} async-done(((bf16[256,1408]{1,0:T(8,128)(2,1)}), bf16[2048,1408]{1,0:T(8,128)(2,1)}) %all-gather.15.cloned.1.call-update) | async-done | bytes 5767184 | tf_op jit(solution)/shard_map/all_gather | solution.py:24
  506.7 93.4 %all-gather.17.cloned.1.call-done = bf16[1408,2048]{1,0:T(8,128)(2,1)} async-done(((bf16[1408,256]{1,0:T(8,128)(2,1)}), bf16[1408,2048]{1,0:T(8,128)(2,1)}) %all-gather.17.cloned.1.call-update) | async-done | bytes 5767184 | tf_op jit(solution)/shard_map/all_gather | solution.py:31
  600.1 9.7 %convolution_convert_fusion = bf16[320,2048]{1,0:T(8,128)(2,1)} fusion(bf16[1408,2048]{1,0:T(8,128)(2,1)} %all-gather.17.cloned.1.call-done, bf16[320,2048]{1,0:T(8,128)(2,1)S(1)} %add_convert_fusion.1, bf16[2048,1408]{1,0:T(8,128)(2,1)} %all-gather.15.cloned.1.call-done, f32[320,1408]{1,0:T(8,128)S(1)} %fusion.8), kind=kOutput, calls=%fused_computation.2 | convolution fusion | flops 3694346240 | bytes 15958016 | tf_op jit(solution)/shard_map/dot_general | solution.py:29
  609.8 18.2 %all-reduce.5.cloned.1.call-done = bf16[320,2048]{1,0:T(8,128)(2,1)} async-done(((bf16[320,2048]{1,0:T(8,128)(2,1)}), bf16[320,2048]{1,0:T(8,128)(2,1)}) %all-reduce.5.cloned.1.call-update) | async-done | bytes 1310736 | tf_op jit(solution)/shard_map/psum | solution.py:40
  628.0 2.0 fusion.4
  630.0 0.8 multiply_reduce_fusion
  630.9 1.9 add_convert_fusion
  (30 shorter events, 0.2 us)
Async XLA Ops:
  6.5 98.0 %all-gather.7.cloned.1.call-start = ((), (), s32[]{:S(2)}) async-start(), calls=%async_computation | async-start | bytes 6488064 | tf_op jit(solution)/shard_map/all_gather | solution.py:23
  7.3 190.7 %all-gather.11.cloned.1.call-start = ((), (), s32[]{:S(2)}) async-start(), calls=%async_computation.2 | async-start | bytes 6488064 | tf_op jit(solution)/shard_map/all_gather | solution.py:31
  8.0 282.7 %all-gather.9.cloned.1.call-start = ((), (), s32[]{:S(2)}) async-start(), calls=%async_computation.1 | async-start | bytes 6488064 | tf_op jit(solution)/shard_map/all_gather | solution.py:24
  8.7 281.9 %copy-start.2 = (bf16[320,2048]{1,0:T(8,128)(2,1)S(1)}, bf16[320,2048]{1,0:T(8,128)(2,1)}, u32[]{:S(2)}) copy-start(bf16[320,2048]{1,0:T(8,128)(2,1)} %param.14) | copy-start | bytes 3932164
  8.8 309.8 %all-reduce.3.cloned.1.call-start = ((), (), s32[]{:S(2)}) async-start(), calls=%async_computation.3 | async-start | bytes 2621440 | tf_op jit(solution)/shard_map/psum | solution.py:40
  300.4 113.8 %all-gather.13.cloned.1.call-start = ((), (), s32[]{:S(2)}) async-start(), calls=%async_computation.4 | async-start | bytes 6488064 | tf_op jit(solution)/shard_map/all_gather | solution.py:23
  301.0 205.8 %all-gather.15.cloned.1.call-start = ((), (), s32[]{:S(2)}) async-start(), calls=%async_computation.5 | async-start | bytes 6488064 | tf_op jit(solution)/shard_map/all_gather | solution.py:24
  301.5 298.6 %all-gather.17.cloned.1.call-start = ((), (), s32[]{:S(2)}) async-start(), calls=%async_computation.6 | async-start | bytes 6488064 | tf_op jit(solution)/shard_map/all_gather | solution.py:31
  301.6 19.9 %copy-start.4 = (f32[2048]{0:T(1024)S(1)}, f32[2048]{0:T(1024)}, u32[]{:S(2)}) copy-start(f32[2048]{0:T(1024)} %param.23) | copy-start | bytes 24580
  301.6 19.9 %copy-start.5 = (f32[2048]{0:T(1024)S(1)}, f32[2048]{0:T(1024)}, u32[]{:S(2)}) copy-start(f32[2048]{0:T(1024)} %param.22) | copy-start | bytes 24580
  302.3 19.2 %copy-start.1 = (bf16[320,2048]{1,0:T(8,128)(2,1)S(1)}, bf16[320,2048]{1,0:T(8,128)(2,1)}, u32[]{:S(2)}) copy-start(bf16[320,2048]{1,0:T(8,128)(2,1)} %param.15) | copy-start | bytes 3932164
  302.3 325.7 %all-reduce.5.cloned.1.call-start = ((), (), s32[]{:S(2)}) async-start(), calls=%async_computation.7 | async-start | bytes 2621440 | tf_op jit(solution)/shard_map/psum | solution.py:40
  318.6 2.0 copy-start.3
  322.8 0.7 copy-start.6
  322.8 0.7 copy-start.7
  609.8 21.0 %copy-start.8 = (f32[2048]{0:T(1024)S(1)}, f32[2048]{0:T(1024)}, u32[]{:S(2)}) copy-start(f32[2048]{0:T(1024)} %param.27) | copy-start | bytes 24580
  609.8 21.0 %copy-start.9 = (f32[2048]{0:T(1024)S(1)}, f32[2048]{0:T(1024)}, u32[]{:S(2)}) copy-start(f32[2048]{0:T(1024)} %param.26) | copy-start | bytes 24580
  628.0 2.0 copy-start
Sparse Core Ops, SparseCore 0:
  9.5 95.0 all-gather.6
  106.6 91.3 all-gather.10
  200.2 90.4 all-gather.8
  300.5 18.0 all-reduce.2
  320.6 93.4 all-gather.12
  416.2 90.4 all-gather.14
  508.8 91.2 all-gather.16
  609.9 18.0 all-reduce.4
where the time goes:
time: 640 us
  waiting for transfers between devices  586 us (92%)
  matrix products  29.4 us (5%)
  between operations  13.6 us (2%)
  other arithmetic  10.4 us (2%)
    all_gather x2, waiting for transfers between devices, project_in(): lax.all_gather(gate_weight, 'fs', axis=0, tiled=True)  186 us
    all_gather x2, waiting for transfers between devices, project_out(): lax.all_gather(down_weight, 'fs', axis=1, tiled=True)  182 us
    all_gather x2, waiting for transfers between devices, project_in(): lax.all_gather(up_weight, 'fs', axis=0, tiled=True)  180 us
    psum x2, waiting for transfers between devices, half_step(): summed = lax.psum(partials.astype(jnp.bfloat16), 'tp')  34.3 us
    dot_general x2, matrix products, project_out(): jnp.dot(hidden, lax.all_gather(down_weight, 'fs', axis=1, tiled=True), pr...  19.3 us
  transfers between devices with their start and end apart: 8, of which 8 were waited for; matrix products, arithmetic and copies ran while one was open for 2% of the time, Pallas kernels for 0%

commit v1 on v0

--- a/solution.py
+++ b/solution.py
@@ -6,6 +6,19 @@
 
 residual_scale = math.sqrt(2.0)
 norm_eps = 1e-05
+
+
+def ring_gather(x, axis, dim):
+    ways = lax.axis_size(axis)
+    up = [(d, (d + 1) % ways) for d in range(ways)]
+    down = [(d, (d - 1) % ways) for d in range(ways)]
+    earlier, later = ([x], [x])
+    for _ in range(ways // 2):
+        earlier.append(lax.ppermute(earlier[-1], axis, up))
+    for _ in range((ways - 1) // 2):
+        later.append(lax.ppermute(later[-1], axis, down))
+    line = jnp.concatenate([*earlier[::-1], *later[1:]], axis=dim)
+    return jnp.roll(line, (lax.axis_index(axis) - ways // 2) * x.shape[dim], axis=dim)
 
 
 def normalize(summed, scaling, offset):
@@ -20,7 +33,7 @@
 
 def project_in(inputs, gate_weight, up_weight):
     return (
-        add_columns(inputs, lax.all_gather(gate_weight, "fs", axis=0, tiled=True)),
+        add_columns(inputs, ring_gather(gate_weight, "fs", 0)),
         add_columns(inputs, lax.all_gather(up_weight, "fs", axis=0, tiled=True)),
     )
 

time: 640 us -> 592 us (0.925)
  waiting for transfers between devices: 586 us -> 455 us
  starting transfers between devices: 0.45 us -> 64.2 us
  local copies, waits for them, and re-layouts: 0.05 us -> 17.2 us
    ppermute x0 -> x14, waiting for transfers between devices: none -> 237 us  [the longest x8 237 us: ring_gather(): earlier.append(lax.ppermute(earlier[-1], axis, up))]
    all_gather x2 -> x0, waiting for transfers between devices: 186 us -> none  [project_in(): lax.all_gather(gate_weight, 'fs', axis=0, tiled=True)]
    all_gather x2, waiting for transfers between devices: 180 us -> 19.3 us  [project_in(): lax.all_gather(up_weight, 'fs', axis=0, tiled=True)]
    ppermute x0 -> x14, starting transfers between devices: none -> 64 us  [the longest x6 50.7 us: ring_gather(): later.append(lax.ppermute(later[-1], axis, down))]
    psum x2, waiting for transfers between devices: 34.3 us -> 18.2 us  [half_step(): summed = lax.psum(partials.astype(jnp.bfloat16), 'tp')]
    unnamed x20 -> x38, local copies, waits for them, and re-layouts: 0.05 us -> 15.3 us
  transfers between devices with their start and end apart: 8 -> 20, of which waited for: 8 -> 13; matrix products, arithmetic and copies ran while one was open for 2% -> 5% of each run, Pallas kernels for 0% -> 0%
where the time goes in v1:
time: 592 us
  waiting for transfers between devices  455 us (77%)
  starting transfers between devices  64.2 us (11%)
  matrix products  31.2 us (5%)
  local copies, waits for them, and re-layouts  17.2 us (3%)
  between operations  13.6 us (2%)
  other arithmetic  10.4 us (2%)
    ppermute x8, waiting for transfers between devices, ring_gather(): earlier.append(lax.ppermute(earlier[-1], axis, up))  237 us
    all_gather x2, waiting for transfers between devices, project_out(): lax.all_gather(down_weight, 'fs', axis=1, tiled=True)  179 us
    ppermute x6, starting transfers between devices, ring_gather(): later.append(lax.ppermute(later[-1], axis, down))  50.7 us
    dot_general x2, matrix products, project_out(): jnp.dot(hidden, lax.all_gather(down_weight, 'fs', axis=1, tiled=True), pr...  21.5 us
    all_gather x2, waiting for transfers between devices, project_in(): lax.all_gather(up_weight, 'fs', axis=0, tiled=True)  19.3 us
    psum x2, waiting for transfers between devices, half_step(): summed = lax.psum(partials.astype(jnp.bfloat16), 'tp')  18.2 us
    unnamed x38, local copies, waits for them, and re-layouts  15.3 us
    ppermute x8, starting transfers between devices, ring_gather(): earlier.append(lax.ppermute(earlier[-1], axis, up))  13.4 us
  transfers between devices with their start and end apart: 20, of which 13 were waited for; matrix products, arithmetic and copies ran while one was open for 5% of the time, Pallas kernels for 0%

profile of v1, /device:TPU:0, one launch (start us, length us, event | category | flops | bytes accessed | tf_op | source)
XLA Modules:
  0.0 592.0 jit_solution(7408308319202359925)
XLA Ops:
  8.1 3.0 collective-permute-start
  11.1 24.5 %collective-permute-done = bf16[256,1408]{1,0:T(8,128)(2,1)S(1)} collective-permute-done((bf16[256,1408]{1,0:T(8,128)(2,1)}, bf16[256,1408]{1,0:T(8,128)(2,1)S(1)}, u32[]{:S(2)}, u32[]{:S(2)}) %collective-permute-start) | collective-permute-done | bytes 720928 | tf_op jit(solution)/shard_map/ppermute | solution.py:17
  36.1 4.3 collective-permute-start.4
  40.3 28.9 %collective-permute-done.1 = bf16[256,1408]{1,0:T(8,128)(2,1)S(1)} collective-permute-done((bf16[256,1408]{1,0:T(8,128)(2,1)S(1)}, bf16[256,1408]{1,0:T(8,128)(2,1)S(1)}, u32[]{:S(2)}, u32[]{:S(2)}) %collective-permute-start.1) | collective-permute-done | bytes 720928 | tf_op jit(solution)/shard_map/ppermute | solution.py:17
  69.2 13.8 %collective-permute-start.5 = (bf16[256,1408]{1,0:T(8,128)(2,1)S(1)}, bf16[256,1408]{1,0:T(8,128)(2,1)S(1)}, u32[]{:S(2)}, u32[]{:S(2)}) collective-permute-start(bf16[256,1408]{1,0:T(8,128)(2,1)S(1)} %collective-permute-done.4), channel_id=1, source_target_pairs={{0,14},{2,0},{4,2},{6,4},{8,6},{10,8},{12,10},{14,12},{1,15},{3,1}... | collective-permute-start | bytes 2162696 | tf_op jit(solution)/shard_map/ppermute | solution.py:19
  83.0 32.0 %collective-permute-done.2 = bf16[256,1408]{1,0:T(8,128)(2,1)} collective-permute-done((bf16[256,1408]{1,0:T(8,128)(2,1)S(1)}, bf16[256,1408]{1,0:T(8,128)(2,1)}, u32[]{:S(2)}, u32[]{:S(2)}) %collective-permute-start.2) | collective-permute-done | bytes 720928 | tf_op jit(solution)/shard_map/ppermute | solution.py:17
  115.0 2.6 collective-permute-start.3
  117.6 24.3 %collective-permute-start.6 = (bf16[256,1408]{1,0:T(8,128)(2,1)S(1)}, bf16[256,1408]{1,0:T(8,128)(2,1)S(1)}, u32[]{:S(2)}, u32[]{:S(2)}) collective-permute-start(bf16[256,1408]{1,0:T(8,128)(2,1)S(1)} %collective-permute-done.5), channel_id=1, source_target_pairs={{0,14},{2,0},{4,2},{6,4},{8,6},{10,8},{12,10},{14,12},{1,15},{3,1}... | collective-permute-start | bytes 2162696 | tf_op jit(solution)/shard_map/ppermute | solution.py:19
  141.9 19.6 %collective-permute-done.3 = bf16[256,1408]{1,0:T(8,128)(2,1)} collective-permute-done((bf16[256,1408]{1,0:T(8,128)(2,1)}, bf16[256,1408]{1,0:T(8,128)(2,1)}, u32[]{:S(2)}, u32[]{:S(2)}) %collective-permute-start.3) | collective-permute-done | bytes 720928 | tf_op jit(solution)/shard_map/ppermute | solution.py:17
  161.5 2.1 constant_dynamic-update-slice_fusion.7
  163.6 2.0 constant_dynamic-update-slice_fusion.6
  171.2 7.7 %all-gather.5.cloned.1.call-done = bf16[2048,1408]{1,0:T(8,128)(2,1)} async-done(((bf16[256,1408]{1,0:T(8,128)(2,1)}), bf16[2048,1408]{1,0:T(8,128)(2,1)}) %all-gather.5.cloned.1.call-update) | async-done | bytes 5767184 | tf_op jit(solution)/shard_map/all_gather | solution.py:37
  178.9 4.8 fusion.32
  183.7 90.2 %all-gather.7.cloned.1.call-done = bf16[1408,2048]{1,0:T(8,128)(2,1)} async-done(((bf16[1408,256]{1,0:T(8,128)(2,1)}), bf16[1408,2048]{1,0:T(8,128)(2,1)}) %all-gather.7.cloned.1.call-update) | async-done | bytes 5767184 | tf_op jit(solution)/shard_map/all_gather | solution.py:44
  273.9 10.8 %convolution_convert_fusion.1 = bf16[320,2048]{1,0:T(8,128)(2,1)} fusion(bf16[1408,2048]{1,0:T(8,128)(2,1)} %all-gather.7.cloned.1.call-done, f32[320,1408]{1,0:T(8,128)S(1)} %fusion.32, bf16[320,2048]{1,0:T(8,128)(2,1)S(1)} %copy-done.2, s32[]{:T(128)S(6)} %select_n.13, bf16[2048,1408]{1,0:T(8,128)(2,1)} %constant_dynamic-update-slice_fusion), kind=kOutput, calls=%fused_computation.10 | convolution fusion | flops 3705880576 | bytes 15958020 | tf_op jit(solution)/shard_map/dot_general | solution.py:42
  286.0 1.5 collective-permute-start.7
  287.4 18.4 %collective-permute-done.7 = bf16[256,1408]{1,0:T(8,128)(2,1)S(1)} collective-permute-done((bf16[256,1408]{1,0:T(8,128)(2,1)S(1)}, bf16[256,1408]{1,0:T(8,128)(2,1)S(1)}, u32[]{:S(2)}, u32[]{:S(2)}) %collective-permute-start.7) | collective-permute-done | bytes 720928 | tf_op jit(solution)/shard_map/ppermute | solution.py:17
  305.8 4.7 collective-permute-start.11
  310.5 32.7 %collective-permute-done.8 = bf16[256,1408]{1,0:T(8,128)(2,1)S(1)} collective-permute-done((bf16[256,1408]{1,0:T(8,128)(2,1)S(1)}, bf16[256,1408]{1,0:T(8,128)(2,1)S(1)}, u32[]{:S(2)}, u32[]{:S(2)}) %collective-permute-start.8) | collective-permute-done | bytes 720928 | tf_op jit(solution)/shard_map/ppermute | solution.py:17
  343.2 2.5 collective-permute-start.9
  345.7 2.2 collective-permute-start.12
  347.9 38.5 %collective-permute-done.9 = bf16[256,1408]{1,0:T(8,128)(2,1)S(1)} collective-permute-done((bf16[256,1408]{1,0:T(8,128)(2,1)S(1)}, bf16[256,1408]{1,0:T(8,128)(2,1)S(1)}, u32[]{:S(2)}, u32[]{:S(2)}) %collective-permute-start.9) | collective-permute-done | bytes 720928 | tf_op jit(solution)/shard_map/ppermute | solution.py:17
  386.4 3.3 collective-permute-start.10
  391.1 42.0 %collective-permute-done.10 = bf16[256,1408]{1,0:T(8,128)(2,1)S(1)} collective-permute-done((bf16[256,1408]{1,0:T(8,128)(2,1)S(1)}, bf16[256,1408]{1,0:T(8,128)(2,1)S(1)}, u32[]{:S(2)}, u32[]{:S(2)}) %collective-permute-start.10) | collective-permute-done | bytes 720928 | tf_op jit(solution)/shard_map/ppermute | solution.py:17
  440.6 2.1 fusion.14
  446.4 11.6 %all-gather.9.cloned.1.call-done = bf16[2048,1408]{1,0:T(8,128)(2,1)} async-done(((bf16[256,1408]{1,0:T(8,128)(2,1)}), bf16[2048,1408]{1,0:T(8,128)(2,1)}) %all-gather.9.cloned.1.call-update) | async-done | bytes 5767184 | tf_op jit(solution)/shard_map/all_gather | solution.py:37
  458.0 4.8 fusion.33
  462.8 88.6 %all-gather.11.cloned.1.call-done = bf16[1408,2048]{1,0:T(8,128)(2,1)} async-done(((bf16[1408,256]{1,0:T(8,128)(2,1)}), bf16[1408,2048]{1,0:T(8,128)(2,1)}) %all-gather.11.cloned.1.call-update) | async-done | bytes 5767184 | tf_op jit(solution)/shard_map/all_gather | solution.py:44
  551.4 10.8 %convolution_convert_fusion = bf16[320,2048]{1,0:T(8,128)(2,1)} fusion(bf16[1408,2048]{1,0:T(8,128)(2,1)} %all-gather.11.cloned.1.call-done, f32[320,1408]{1,0:T(8,128)S(1)} %fusion.33, bf16[320,2048]{1,0:T(8,128)(2,1)S(1)} %add_convert_fusion.1, s32[]{:T(128)S(6)} %select_n.13, bf16[2048,1408]{1,0:T(8,128)(2,1)} %constant_dynamic-update-slice_fusion.8), kind=kOutput, calls=%fused_computation.9 | convolution fusion | flops 3705880576 | bytes 15958020 | tf_op jit(solution)/shard_map/dot_general | solution.py:42
  562.2 18.2 %all-reduce.5.cloned.1.call-done = bf16[320,2048]{1,0:T(8,128)(2,1)} async-done(((bf16[320,2048]{1,0:T(8,128)(2,1)}), bf16[320,2048]{1,0:T(8,128)(2,1)}) %all-reduce.5.cloned.1.call-update) | async-done | bytes 1310736 | tf_op jit(solution)/shard_map/psum | solution.py:53
  580.4 2.0 fusion.15
  583.2 1.9 add_convert_fusion
  (72 shorter events, 22.0 us)
Async XLA Ops:
  6.5 172.4 %all-gather.5.cloned.1.call-start = ((), (), s32[]{:S(2)}) async-start(), calls=%async_computation | async-start | bytes 6488064 | tf_op jit(solution)/shard_map/all_gather | solution.py:37
  7.3 266.7 %all-gather.7.cloned.1.call-start = ((), (), s32[]{:S(2)}) async-start(), calls=%async_computation.1 | async-start | bytes 6488064 | tf_op jit(solution)/shard_map/all_gather | solution.py:44
  8.0 432.6 %all-reduce.3.cloned.1.call-start = ((), (), s32[]{:S(2)}) async-start(), calls=%async_computation.2 | async-start | bytes 2621440 | tf_op jit(solution)/shard_map/psum | solution.py:53
  8.1 27.6 %collective-permute-start = (bf16[256,1408]{1,0:T(8,128)(2,1)}, bf16[256,1408]{1,0:T(8,128)(2,1)S(1)}, u32[]{:S(2)}, u32[]{:S(2)}) collective-permute-start(bf16[256,1408]{1,0:T(8,128)(2,1)} %param.18), channel_id=1, source_target_pairs={{0,2},{2,4},{4,6},{6,8},{8,10},{10,12},{12,14},{14,0},{1,3},{3,5},... | collective-permute-start | bytes 2162696 | tf_op jit(solution)/shard_map/ppermute | solution.py:17
  35.6 33.6 %collective-permute-start.1 = (bf16[256,1408]{1,0:T(8,128)(2,1)S(1)}, bf16[256,1408]{1,0:T(8,128)(2,1)S(1)}, u32[]{:S(2)}, u32[]{:S(2)}) collective-permute-start(bf16[256,1408]{1,0:T(8,128)(2,1)S(1)} %collective-permute-done), channel_id=1, source_target_pairs={{0,2},{2,4},{4,6},{6,8},{8,10},{10,12},{12,14},{14,0},{1,3},{3,5},... | collective-permute-start | bytes 2162696 | tf_op jit(solution)/shard_map/ppermute | solution.py:17
  36.1 33.2 %collective-permute-start.4 = (bf16[256,1408]{1,0:T(8,128)(2,1)}, bf16[256,1408]{1,0:T(8,128)(2,1)S(1)}, u32[]{:S(2)}, u32[]{:S(2)}) collective-permute-start(bf16[256,1408]{1,0:T(8,128)(2,1)} %param.18), channel_id=1, source_target_pairs={{0,14},{2,0},{4,2},{6,4},{8,6},{10,8},{12,10},{14,12},{1,15},{3,1}... | collective-permute-start | bytes 2162696 | tf_op jit(solution)/shard_map/ppermute | solution.py:19
  69.2 45.8 %collective-permute-start.2 = (bf16[256,1408]{1,0:T(8,128)(2,1)S(1)}, bf16[256,1408]{1,0:T(8,128)(2,1)}, u32[]{:S(2)}, u32[]{:S(2)}) collective-permute-start(bf16[256,1408]{1,0:T(8,128)(2,1)S(1)} %collective-permute-done.1), channel_id=1, source_target_pairs={{0,2},{2,4},{4,6},{6,8},{8,10},{10,12},{12,14},{14,0},{1,3},{3,5},... | collective-permute-start | bytes 2162696 | tf_op jit(solution)/shard_map/ppermute | solution.py:17
  69.2 48.3 %collective-permute-start.5 = (bf16[256,1408]{1,0:T(8,128)(2,1)S(1)}, bf16[256,1408]{1,0:T(8,128)(2,1)S(1)}, u32[]{:S(2)}, u32[]{:S(2)}) collective-permute-start(bf16[256,1408]{1,0:T(8,128)(2,1)S(1)} %collective-permute-done.4), channel_id=1, source_target_pairs={{0,14},{2,0},{4,2},{6,4},{8,6},{10,8},{12,10},{14,12},{1,15},{3,1}... | collective-permute-start | bytes 2162696 | tf_op jit(solution)/shard_map/ppermute | solution.py:19
  115.0 46.5 %collective-permute-start.3 = (bf16[256,1408]{1,0:T(8,128)(2,1)}, bf16[256,1408]{1,0:T(8,128)(2,1)}, u32[]{:S(2)}, u32[]{:S(2)}) collective-permute-start(bf16[256,1408]{1,0:T(8,128)(2,1)} %collective-permute-done.2), channel_id=1, source_target_pairs={{0,2},{2,4},{4,6},{6,8},{8,10},{10,12},{12,14},{14,0},{1,3},{3,5},... | collective-permute-start | bytes 2162696 | tf_op jit(solution)/shard_map/ppermute | solution.py:17
  117.6 49.9 %copy-start.4 = (bf16[256,1408]{1,0:T(8,128)(2,1)S(1)}, bf16[256,1408]{1,0:T(8,128)(2,1)}, u32[]{:S(2)}) copy-start(bf16[256,1408]{1,0:T(8,128)(2,1)} %param.18) | copy-start | bytes 2162692
  117.6 52.6 %collective-permute-start.6 = (bf16[256,1408]{1,0:T(8,128)(2,1)S(1)}, bf16[256,1408]{1,0:T(8,128)(2,1)S(1)}, u32[]{:S(2)}, u32[]{:S(2)}) collective-permute-start(bf16[256,1408]{1,0:T(8,128)(2,1)S(1)} %collective-permute-done.5), channel_id=1, source_target_pairs={{0,14},{2,0},{4,2},{6,4},{8,6},{10,8},{12,10},{14,12},{1,15},{3,1}... | collective-permute-start | bytes 2162696 | tf_op jit(solution)/shard_map/ppermute | solution.py:19
  167.5 11.4 %copy-start.2 = (bf16[320,2048]{1,0:T(8,128)(2,1)S(1)}, bf16[320,2048]{1,0:T(8,128)(2,1)}, u32[]{:S(2)}) copy-start(bf16[320,2048]{1,0:T(8,128)(2,1)} %param.16) | copy-start | bytes 3932164
  284.7 1.2 copy-start.5
  284.7 173.2 %all-gather.9.cloned.1.call-start = ((), (), s32[]{:S(2)}) async-start(), calls=%async_computation.3 | async-start | bytes 6488064 | tf_op jit(solution)/shard_map/all_gather | solution.py:37
  285.3 266.1 %all-gather.11.cloned.1.call-start = ((), (), s32[]{:S(2)}) async-start(), calls=%async_computation.4 | async-start | bytes 6488064 | tf_op jit(solution)/shard_map/all_gather | solution.py:44
  285.9 294.5 %all-reduce.5.cloned.1.call-start = ((), (), s32[]{:S(2)}) async-start(), calls=%async_computation.5 | async-start | bytes 2621440 | tf_op jit(solution)/shard_map/psum | solution.py:53
  286.0 19.9 %collective-permute-start.7 = (bf16[256,1408]{1,0:T(8,128)(2,1)S(1)}, bf16[256,1408]{1,0:T(8,128)(2,1)S(1)}, u32[]{:S(2)}, u32[]{:S(2)}) collective-permute-start(bf16[256,1408]{1,0:T(8,128)(2,1)S(1)} %copy-done.5), channel_id=1, source_target_pairs={{0,2},{2,4},{4,6},{6,8},{8,10},{10,12},{12,14},{14,0},{1,3},{3,5},... | collective-permute-start | bytes 2162696 | tf_op jit(solution)/shard_map/ppermute | solution.py:17
  305.8 37.4 %collective-permute-start.8 = (bf16[256,1408]{1,0:T(8,128)(2,1)S(1)}, bf16[256,1408]{1,0:T(8,128)(2,1)S(1)}, u32[]{:S(2)}, u32[]{:S(2)}) collective-permute-start(bf16[256,1408]{1,0:T(8,128)(2,1)S(1)} %collective-permute-done.7), channel_id=1, source_target_pairs={{0,2},{2,4},{4,6},{6,8},{8,10},{10,12},{12,14},{14,0},{1,3},{3,5},... | collective-permute-start | bytes 2162696 | tf_op jit(solution)/shard_map/ppermute | solution.py:17
  305.8 39.9 %collective-permute-start.11 = (bf16[256,1408]{1,0:T(8,128)(2,1)S(1)}, bf16[256,1408]{1,0:T(8,128)(2,1)S(1)}, u32[]{:S(2)}, u32[]{:S(2)}) collective-permute-start(bf16[256,1408]{1,0:T(8,128)(2,1)S(1)} %copy-done.5), channel_id=1, source_target_pairs={{0,14},{2,0},{4,2},{6,4},{8,6},{10,8},{12,10},{14,12},{1,15},{3,1}... | collective-permute-start | bytes 2162696 | tf_op jit(solution)/shard_map/ppermute | solution.py:19
  343.2 43.2 %collective-permute-start.9 = (bf16[256,1408]{1,0:T(8,128)(2,1)S(1)}, bf16[256,1408]{1,0:T(8,128)(2,1)S(1)}, u32[]{:S(2)}, u32[]{:S(2)}) collective-permute-start(bf16[256,1408]{1,0:T(8,128)(2,1)S(1)} %collective-permute-done.8), channel_id=1, source_target_pairs={{0,2},{2,4},{4,6},{6,8},{8,10},{10,12},{12,14},{14,0},{1,3},{3,5},... | collective-permute-start | bytes 2162696 | tf_op jit(solution)/shard_map/ppermute | solution.py:17
  345.7 44.1 %collective-permute-start.12 = (bf16[256,1408]{1,0:T(8,128)(2,1)S(1)}, bf16[256,1408]{1,0:T(8,128)(2,1)S(1)}, u32[]{:S(2)}, u32[]{:S(2)}) collective-permute-start(bf16[256,1408]{1,0:T(8,128)(2,1)S(1)} %collective-permute-done.11), channel_id=1, source_target_pairs={{0,14},{2,0},{4,2},{6,4},{8,6},{10,8},{12,10},{14,12},{1,15},{3,1}... | collective-permute-start | bytes 2162696 | tf_op jit(solution)/shard_map/ppermute | solution.py:19
  386.4 46.8 %collective-permute-start.10 = (bf16[256,1408]{1,0:T(8,128)(2,1)S(1)}, bf16[256,1408]{1,0:T(8,128)(2,1)S(1)}, u32[]{:S(2)}, u32[]{:S(2)}) collective-permute-start(bf16[256,1408]{1,0:T(8,128)(2,1)S(1)} %collective-permute-done.9), channel_id=1, source_target_pairs={{0,2},{2,4},{4,6},{6,8},{8,10},{10,12},{12,14},{14,0},{1,3},{3,5},... | collective-permute-start | bytes 2162696 | tf_op jit(solution)/shard_map/ppermute | solution.py:17
  389.7 49.9 %collective-permute-start.13 = (bf16[256,1408]{1,0:T(8,128)(2,1)S(1)}, bf16[256,1408]{1,0:T(8,128)(2,1)S(1)}, u32[]{:S(2)}, u32[]{:S(2)}) collective-permute-start(bf16[256,1408]{1,0:T(8,128)(2,1)S(1)} %collective-permute-done.12), channel_id=1, source_target_pairs={{0,14},{2,0},{4,2},{6,4},{8,6},{10,8},{12,10},{14,12},{1,15},{3,1}... | collective-permute-start | bytes 2162696 | tf_op jit(solution)/shard_map/ppermute | solution.py:19
  440.6 2.9 copy-start.1
  440.6 2.1 copy-start.3
  440.6 2.9 copy-start.6
  440.6 2.9 copy-start.7
  444.8 0.7 copy-start.8
  444.8 0.7 copy-start.9
  562.2 21.0 %copy-start.10 = (f32[2048]{0:T(1024)S(1)}, f32[2048]{0:T(1024)}, u32[]{:S(2)}) copy-start(f32[2048]{0:T(1024)} %param.29) | copy-start | bytes 24580
  562.2 21.0 %copy-start.11 = (f32[2048]{0:T(1024)S(1)}, f32[2048]{0:T(1024)}, u32[]{:S(2)}) copy-start(f32[2048]{0:T(1024)} %param.28) | copy-start | bytes 24580
  580.4 2.0 copy-start
Sparse Core Ops, SparseCore 0:
  9.5 169.3 all-gather.4
  180.9 92.9 all-gather.6
  284.9 18.0 all-reduce.2
  305.0 152.9 all-gather.8
  459.8 91.4 all-gather.10
  562.3 18.0 all-reduce.4
